TPU v7x, 32 devices: a whole 2x2x4 slice. The times are simulated.
32 devices in a mesh: ep: 8 (over z, y), tp: 4 (over x, core).
Axes of the slice: x: 2, y: 2, z: 4, core: 2. Of those that a mesh axis runs over, the one named last changes fastest.
Arguments:
- query_rows: bfloat16 [4096, 1024], P('ep', 'tp'), may hold values from -60 to 60
- key_rows: bfloat16 [4096, 1024], P('ep', 'tp'), may hold values from -6 to 6
- value_rows: bfloat16 [4096, 1024], P('ep', 'tp'), may hold values from -6 to 6
- lambdas: float32 [8], P('tp'), may hold values from 0.3 to 0.8
- out_gain: float32 [128], replicated, may hold values from 0.1 to 1.9
- out_weight: bfloat16 [1024, 2048], P('tp'), may hold values from -0.1875 to 0.1875
- tokens: bfloat16 [4096, 2048], P(('ep', 'tp')), may hold values from -6 to 6
- norm_gain: float32 [2048], replicated, may hold values from 0.1 to 1.9
- group_ids: int32 [4096], P(('ep', 'tp')), may hold values from 0 to 3, as said below
- inner_ids: int32 [4096, 2], P(('ep', 'tp')), may hold values from 0 to 1, as said below
- route_weights: float32 [4096, 2], P(('ep', 'tp')), may hold values from 0.2 to 1
- gate_weight: bfloat16 [8, 2048, 1024], P('ep', None, 'tp'), may hold values from -0.125 to 0.125
- up_weight: bfloat16 [8, 2048, 1024], P('ep', None, 'tp'), may hold values from -0.125 to 0.125
- down_weight: bfloat16 [8, 1024, 2048], P('ep', 'tp'), may hold values from -0.1875 to 0.1875
Outputs:
- attended: bfloat16 [4096, 2048], P(('ep', 'tp'))
- combined: bfloat16 [4096, 2048], P(('ep', 'tp'))
Inputs may be any that keep to these rules, and one draw needn't show every extreme that they name: In the 128 rows of one device no expert group_ids * 2 + inner_ids is named more than 40 times; some expert is named exactly 40 times in the rows of every device. `inner_ids`: the 2 entries of a row are different.
All inputs are finite; a program needn't handle non-finite values.
Results may differ from a plain program's by a relative error of at most 0.013.
Values may be sent and summed in bfloat16 or wider, within the bound.
A program may use at most 128 MiB of HBM per device.

v0:
```python
import jax
import jax.numpy as jnp
from jax import lax
from jax.sharding import PartitionSpec as P

GROUPS = 4
eps = 1e-06
neg_big = -1e30


def body(
    query_rows,
    key_rows,
    value_rows,
    lambdas,
    out_gain,
    out_weight,
    tokens,
    norm_gain,
    group_ids,
    inner_ids,
    route_weights,
    gate_weight,
    up_weight,
    down_weight,
):
    seg_rows = query_rows.shape[0]
    heads_here = lambdas.shape[0]
    value_dim = out_gain.shape[0]
    query_dim = query_rows.shape[1] // (2 * heads_here)
    tok_dev = tokens.shape[0]
    model_width = tokens.shape[1]
    topk_count = inner_ids.shape[1]
    experts = lax.axis_size("ep")
    ep_index = lax.axis_index("ep")
    group_size = experts // GROUPS
    capacity = 5 * tok_dev * topk_count // (4 * experts)
    count = query_rows.shape[0]
    query_groups = (
        (
            query_rows.reshape(count, heads_here, 2, query_dim).transpose(1, 2, 0, 3),
            ep_index * seg_rows + jnp.arange(seg_rows, dtype=jnp.int32),
        ),
    )
    score_scale = query_dim ** (-0.5)

    def one_map(state, query_map, key_map, value_blk, allowed):
        top_old, total_old, accum_old = state
        scores = (
            jnp.einsum("hqd,hdk->hqk", query_map, key_map, preferred_element_type=jnp.float32)
            * score_scale
        )
        scores = jnp.where(allowed[None, :, :], scores, neg_big)
        top_new = jnp.maximum(top_old, jnp.max(scores, axis=2))
        exps = jnp.where(allowed[None, :, :], jnp.exp(scores - top_new[:, :, None]), 0.0)
        fade = jnp.exp(top_old - top_new)
        total_new = total_old * fade + jnp.sum(exps, axis=2)
        accum_new = accum_old * fade[:, :, None] + jnp.einsum(
            "hqk,hdk->hqd", exps.astype(jnp.bfloat16), value_blk, preferred_element_type=jnp.float32
        )
        return (top_new, total_new, accum_new)

    def key_block(running, query_part, query_pos, key_blk, value_blk, key_start):
        key_pos = key_start + jnp.arange(key_blk.shape[3], dtype=jnp.int32)
        allowed = key_pos[None, :] <= query_pos[:, None]
        first_state = one_map(running[:3], query_part[:, 0], key_blk[:, 0], value_blk, allowed)
        second_state = one_map(running[3:], query_part[:, 1], key_blk[:, 1], value_blk, allowed)
        return first_state + second_state

    def initial(rows):
        top_init = jnp.full((heads_here, rows), neg_big, jnp.float32)
        total_init = jnp.zeros((heads_here, rows), jnp.float32)
        accum_init = jnp.zeros((heads_here, rows, value_dim), jnp.float32)
        return (top_init, total_init, accum_init, top_init, total_init, accum_init)

    init_state = tuple((initial(group[1].shape[0]) for group in query_groups))
    key_cols = key_rows.T
    value_cols = value_rows.T
    key_piece = lax.all_gather(key_cols, "ep", axis=1, tiled=True)
    value_piece = lax.all_gather(value_cols, "ep", axis=1, tiled=True)
    shard_count = key_piece.shape[1] // seg_rows
    stride = max(1, 2048 // seg_rows)
    while shard_count % stride:
        stride -= 1
    block_rows = stride * seg_rows
    turns = shard_count // stride

    def advance(step_num, states):
        key_start = step_num * block_rows
        key_blk = lax.dynamic_slice_in_dim(key_piece, step_num * block_rows, block_rows, 1).reshape(
            heads_here, 2, query_dim, block_rows
        )
        value_blk = lax.dynamic_slice_in_dim(
            value_piece, step_num * block_rows, block_rows, 1
        ).reshape(heads_here, value_dim, block_rows)
        updated = []
        for group, state in zip(query_groups, states):
            query_part, query_pos = group

            def apply_block(inside, query_part=query_part, query_pos=query_pos):
                return key_block(inside, query_part, query_pos, key_blk, value_blk, key_start)

            updated.append(
                lax.cond(key_start <= query_pos[-1], apply_block, lambda inside: inside, state)
            )
        return tuple(updated)

    folded = lax.fori_loop(0, turns, advance, init_state)
    state = folded[0]
    first_out = state[2] / state[1][:, :, None]
    second_out = state[5] / state[4][:, :, None]
    heads_out = first_out - lambdas[:, None, None] * second_out
    mean_sq = jnp.mean(heads_out * heads_out, axis=2, keepdims=True)
    normed_part = (heads_out * lax.rsqrt(mean_sq + eps) * out_gain).astype(jnp.bfloat16)
    rows = state[2].shape[1]
    normed_heads = normed_part.transpose(1, 0, 2).reshape(rows, heads_here * value_dim)
    tok_wide = tokens.astype(jnp.float32)
    normed = (
        tok_wide * lax.rsqrt(jnp.mean(tok_wide * tok_wide, axis=1, keepdims=True) + eps) * norm_gain
    ).astype(jnp.bfloat16)
    target = (group_ids[:, None] * group_size + inner_ids).reshape(-1)
    labels = jnp.arange(experts, dtype=jnp.int32)
    onehot = (target[:, None] == labels[None, :]).astype(jnp.int32)
    slot_rank = jnp.sum((jnp.cumsum(onehot, axis=0) - 1) * onehot, axis=1)
    slot_of = target * capacity + slot_rank
    slot_ids = jnp.arange(experts * capacity, dtype=jnp.int32)
    placing = jnp.any(
        (slot_of[:, None] == slot_ids[None, :]).reshape(tok_dev, topk_count, experts * capacity),
        axis=1,
    ).astype(jnp.bfloat16)
    outgoing = jnp.einsum("ts,td->sd", placing, normed, preferred_element_type=jnp.float32).astype(
        jnp.bfloat16
    )
    arrived = lax.all_to_all(outgoing, "ep", split_axis=0, concat_axis=0, tiled=True)
    gate_all, up_all, down_all, out_all = (
        lax.all_gather(gate_weight, "tp", axis=2, tiled=True),
        lax.all_gather(up_weight, "tp", axis=2, tiled=True),
        lax.all_gather(down_weight, "tp", axis=1, tiled=True),
        lax.all_gather(out_weight, "tp", axis=0, tiled=True),
    )
    own_heads = lax.all_to_all(normed_heads, "tp", split_axis=0, concat_axis=1, tiled=True)
    attended = jnp.dot(own_heads, out_all, preferred_element_type=jnp.float32).astype(jnp.bfloat16)
    gate_pre = jnp.dot(arrived, gate_all[0], preferred_element_type=jnp.float32)
    up_pre = jnp.dot(arrived, up_all[0], preferred_element_type=jnp.float32)
    hidden = (jax.nn.silu(gate_pre) * up_pre).astype(jnp.bfloat16)
    results = jnp.dot(hidden, down_all[0], preferred_element_type=jnp.float32).astype(jnp.bfloat16)
    returned = lax.all_to_all(results, "ep", split_axis=0, concat_axis=0, tiled=True)
    picked = returned[slot_of].reshape(tok_dev, topk_count, model_width)
    combined = jnp.sum(picked.astype(jnp.float32) * route_weights[:, :, None], axis=1).astype(
        jnp.bfloat16
    )
    return (attended, combined)


def solution(mesh):
    in_specs = (
        P("ep", "tp"),
        P("ep", "tp"),
        P("ep", "tp"),
        P("tp"),
        P(),
        P("tp", None),
        P(("ep", "tp"), None),
        P(),
        P(("ep", "tp")),
        P(("ep", "tp"), None),
        P(("ep", "tp"), None),
        P("ep", None, "tp"),
        P("ep", None, "tp"),
        P("ep", "tp", None),
    )
    out_specs = (P(("ep", "tp"), None), P(("ep", "tp"), None))
    return jax.shard_map(body, mesh=mesh, in_specs=in_specs, out_specs=out_specs, check_vma=False)
```

profile of v0, /device:TPU:0, one launch (start us, length us, event | category | flops | bytes accessed | tf_op | source)
XLA Modules:
  0.0 298.9 jit_solution(15995786125273280011)
XLA Ops:
  7.3 1.8 copy.38
  9.2 1.8 copy.40
  11.0 0.7 all-gather.13.cloned.1.call-update
  14.0 0.6 reduce-window.6
  15.4 1.7 convolution_convert_fusion
  17.1 7.3 %all-to-all-start.1 = ((bf16[8,40,2048]{2,1,0:T(8,128)(2,1)}), bf16[8,40,2048]{2,1,0:T(8,128)(2,1)}, u32[]{:S(2)}, u32[]{:S(2)}) async-start(bf16[8,40,2048]{2,1,0:T(8,128)(2,1)} %bitcast.18), calls=%async_computation.1 | async-start | bytes 2621440 | tf_op jit(solution)/shard_map/all_to_all | solution.py:134
  24.6 54.4 %all-gather.7.cloned.1.call-done = bf16[256,4096]{1,0:T(8,128)(2,1)} async-done(((bf16[256,512]{1,0:T(8,128)(2,1)}), bf16[256,4096]{1,0:T(8,128)(2,1)}) %all-gather.7.cloned.1.call-update) | async-done | bytes 2097168 | tf_op jit(solution)/shard_map/all_gather | solution.py:79
  79.0 53.0 %all-gather.9.cloned.1.call-done = bf16[256,4096]{1,0:T(8,128)(2,1)} async-done(((bf16[256,512]{1,0:T(8,128)(2,1)}), bf16[256,4096]{1,0:T(8,128)(2,1)}) %all-gather.9.cloned.1.call-update) | async-done | bytes 2097168 | tf_op jit(solution)/shard_map/all_gather | solution.py:80
  132.1 20.8 %while.23 = (s32[]{:T(128)}, f32[2,512]{1,0:T(2,128)S(1)}, f32[2,512]{1,0:T(2,128)S(1)}, f32[2,512,128]{2,1,0:T(8,128)S(1)}, f32[2,512]{1,0:T(2,128)S(1)}, /*ind...) while((s32[]{:T(128)}, f32[2,512]{1,0:T(2,128)S(1)}, ...), condition=%wide.region_7.8_spmd, body=%wide.region_0.7_spmd.sunk | while | flops 1666717696 | bytes 82201008 | solution.py:108
  132.3 0.6 slice.62
  133.5 17.8 %conditional.2 = ((f32[2,512]{1,0:T(2,128)S(1)}, f32[2,512]{1,0:T(2,128)S(1)}, f32[2,512,128]{2,1,0:T(8,128)S(1)}, f32[2,512]{1,0:T(2,128)S(1)}, f32[2,512]{1,0:T(2,128)S(1)}, /*index=5*/f32[2,512,128]{2,1,0:T(8,128)S(1)})) conditional(s32[]{:T(128)} %convert_element_type.97, (f32[2,512]{1,0:T(2,128)S(1)}, f32[2,512]{1,0:T(2,128)S(1)}, ...), branch_computations={%region_1.0_spmd, %region_2.6_spmd} | conditional | flops 1666717696 | bytes 82200704 | solution.py:104
  133.6 0.8 broadcast_compare_fusion
  134.3 1.3 constant_dynamic-slice_fusion.1
  135.6 1.3 fusion.19
  136.9 3.1 %fusion.1 = (f32[2,512]{1,0:T(2,128)S(1)}, f32[2,512]{1,0:T(2,128)S(1)}, f32[2,2048,512]{2,1,0:T(8,128)S(1)}) fusion(pred[512,2048]{0,1:T(8,128)(4,1)S(1)} %broadcast_compare_fusion, f32[2,2048,512]{2,1,0:T(8,128)S(1)} %fusion.19, bf16[2,2,512,64]{2,3,0,1:T(8,128)(2,1)S(1)} %get-tuple-element.315, bf16[2,2,64,2048]{3,2,1,0:T(8,128)(2,1)S(1)} %bitcast.98), kind=kOutput, calls=%fused_computation.6 | convolution fusion | flops 281016320 | bytes 18489344 | tf_op jit(solution)/shard_map/while/body/eval_jaxpr/cond/branch_1_fun/hqd,hdk->hqk/dot_general | solution.py:50
  140.1 4.1 %fusion.5 = (f32[2,512]{1,0:T(2,128)S(1)}, f32[2,512]{1,0:T(2,128)S(1)}) fusion(f32[2,2048,512]{2,1,0:T(8,128)S(1)} %get-tuple-element.406, f32[2,512]{1,0:T(2,128)S(1)} %max.11, pred[512,2048]{0,1:T(8,128)(4,1)S(1)} %broadcast_compare_fusion, f32[2,512]{1,0:T(2,128)S(1)} %max.10, f32[2,2048,512]{2,1,0:T(8,128)S(1)} %fusion.19), kind=kLoop, calls=%fused_computation.10 | loop fusion | flops 20969472 | bytes 17842176 | tf_op jit(solution)/shard_map/while/body/eval_jaxpr/cond/branch_1_fun/reduce_sum | solution.py:57
  144.3 3.5 %fusion.12 = f32[2,512,128]{2,1,0:T(8,128)S(1)} fusion(bf16[2,128,2048]{2,1,0:T(8,128)(2,1)S(1)} %bitcast.99, f32[2,2048,512]{2,1,0:T(8,128)S(1)} %fusion.19, f32[2,512]{1,0:T(2,128)S(1)} %max.10, pred[512,2048]{0,1:T(8,128)(4,1)S(1)} %broadcast_compare_fusion, f32[2,512,128]{2,1,0:T(8,128)S(1)} %get-tuple-element.317, f32[2,512]{1,0:T(2,128)S(1)} %get-tuple-element.408), kind=kOutput, calls=%fused_computation.16 | convolution fusion | flops 547618816 | bytes 11542528 | tf_op jit(solution)/shard_map/while/body/eval_jaxpr/cond/branch_1_fun/hqk,hdk->hqd/dot_general | solution.py:58
  147.8 3.5 %fusion.15 = f32[2,512,128]{2,1,0:T(8,128)S(1)} fusion(bf16[2,128,2048]{2,1,0:T(8,128)(2,1)S(1)} %bitcast.100, f32[2,2048,512]{2,1,0:T(8,128)S(1)} %get-tuple-element.406, f32[2,512]{1,0:T(2,128)S(1)} %max.11, pred[512,2048]{0,1:T(8,128)(4,1)S(1)} %broadcast_compare_fusion, f32[2,512,128]{2,1,0:T(8,128)S(1)} %get-tuple-element.321, ...), kind=kOutput, calls=%fused_computation.17 | convolution fusion | flops 547618816 | bytes 11542528 | tf_op jit(solution)/shard_map/while/body/eval_jaxpr/cond/branch_1_fun/hqk,hdk->hqd/dot_general | solution.py:58
  153.9 0.9 all_to_all.30
  154.8 3.4 %all-to-all-start = ((bf16[4,128,256]{2,1,0:T(8,128)(2,1)}), bf16[4,128,256]{2,1,0:T(8,128)(2,1)S(1)}, u32[]{:S(2)}, u32[]{:S(2)}) async-start(bf16[4,128,256]{2,1,0:T(8,128)(2,1)} %all_to_all.30), calls=%async_computation | async-start | bytes 524288 | tf_op jit(solution)/shard_map/all_to_all | solution.py:141
  158.2 11.4 %all-gather.13.cloned.1.call-done = bf16[1,2048,1024]{2,1,0:T(8,128)(2,1)} async-done(((bf16[1,2048,256]{2,1,0:T(8,128)(2,1)}), bf16[1,2048,1024]{2,1,0:T(8,128)(2,1)}) %all-gather.13.cloned.1.call-update) | async-done | bytes 4194320 | tf_op jit(solution)/shard_map/all_gather | solution.py:136
  169.5 4.1 %fusion.34 = f32[320,1024]{1,0:T(8,128)S(1)} fusion(bf16[320,2048]{1,0:T(8,128)(2,1)} %bitcast.19, bf16[1,2048,1024]{2,1,0:T(8,128)(2,1)} %all-gather.13.cloned.1.call-done), kind=kOutput, calls=%fused_computation.43 | convolution fusion | flops 1342177280 | bytes 6815744 | tf_op jit(solution)/shard_map/dot_general | solution.py:143
  173.7 29.9 %all-gather.17.cloned.1.call-done = bf16[1,1024,2048]{2,1,0:T(8,128)(2,1)} async-done(((bf16[1,256,2048]{2,1,0:T(8,128)(2,1)}), bf16[1,1024,2048]{2,1,0:T(8,128)(2,1)}) %all-gather.17.cloned.1.call-update) | async-done | bytes 4194320 | tf_op jit(solution)/shard_map/all_gather | solution.py:138
  203.6 36.4 %all-gather.15.cloned.1.call-done = bf16[1,2048,1024]{2,1,0:T(8,128)(2,1)} async-done(((bf16[1,2048,256]{2,1,0:T(8,128)(2,1)}), bf16[1,2048,1024]{2,1,0:T(8,128)(2,1)}) %all-gather.15.cloned.1.call-update) | async-done | bytes 4194320 | tf_op jit(solution)/shard_map/all_gather | solution.py:137
  240.0 8.0 %fusion.36 = bf16[320,2048]{1,0:T(8,128)(2,1)} fusion(bf16[1,1024,2048]{2,1,0:T(8,128)(2,1)} %all-gather.17.cloned.1.call-done, bf16[320,2048]{1,0:T(8,128)(2,1)} %bitcast.19, bf16[1,2048,1024]{2,1,0:T(8,128)(2,1)} %all-gather.15.cloned.1.call-done, f32[320,1024]{1,0:T(8,128)S(1)} %fusion.34), kind=kOutput, calls=%fused_computation.46 | convolution fusion | flops 2686976000 | bytes 12320768 | tf_op jit(solution)/shard_map/dot_general | solution.py:146
  248.1 5.5 %all-to-all-start.2 = ((bf16[8,40,2048]{2,1,0:T(8,128)(2,1)}), bf16[8,40,2048]{2,1,0:T(8,128)(2,1)S(1)}, u32[]{:S(2)}, u32[]{:S(2)}) async-start(bf16[8,40,2048]{2,1,0:T(8,128)(2,1)} %bitcast.23), calls=%async_computation.2 | async-start | bytes 2621440 | tf_op jit(solution)/shard_map/all_to_all | solution.py:147
  254.1 21.9 %all-gather.11.cloned.1.call-done = bf16[1024,2048]{1,0:T(8,128)(2,1)} async-done(((bf16[256,2048]{1,0:T(8,128)(2,1)}), bf16[1024,2048]{1,0:T(8,128)(2,1)}) %all-gather.11.cloned.1.call-update) | async-done | bytes 4194320 | tf_op jit(solution)/shard_map/all_gather | solution.py:139
  275.9 3.7 %convolution_convert_fusion.1 = bf16[128,2048]{1,0:T(8,128)(2,1)} fusion(bf16[128,1024]{0,1:T(8,128)(2,1)S(1)} %bitcast.101, bf16[1024,2048]{1,0:T(8,128)(2,1)} %all-gather.11.cloned.1.call-done), kind=kOutput, calls=%fused_computation.47 | convolution fusion | flops 537133056 | bytes 4980736 | tf_op jit(solution)/shard_map/dot_general | solution.py:142
  279.7 5.7 %all-to-all-done.2 = bf16[8,40,2048]{2,1,0:T(8,128)(2,1)S(1)} async-done(((bf16[8,40,2048]{2,1,0:T(8,128)(2,1)}), bf16[8,40,2048]{2,1,0:T(8,128)(2,1)S(1)}, u32[]{:S(2)}, u32[]{:S(2)}) %all-to-all-start.2) | async-done | bytes 1310752 | tf_op jit(solution)/shard_map/all_to_all | solution.py:147
  285.4 1.4 gather_fusion
  286.8 1.3 reshape.164
  288.1 3.9 %multiply_reduce_fusion = bf16[128,2048]{1,0:T(8,128)(2,1)} fusion(f32[128,2,2048]{2,1,0:T(2,128)S(1)} %reshape.164, f32[128,2]{1,0:T(8,128)S(1)} %copy.46), kind=kLoop, calls=%fused_computation.48 | loop fusion | flops 786432 | bytes 2622464 | tf_op jit(solution)/shard_map/reduce_sum | solution.py:149
  (74 shorter events, 5.6 us)
Async XLA Ops:
  7.2 6.3 %copy-start.4 = (s32[128,2]{0,1:T(2,128)S(1)}, s32[128,2]{0,1:T(2,128)}, u32[]{:S(2)}) copy-start(s32[128,2]{0,1:T(2,128)} %param.27) | copy-start | bytes 3076
  7.2 6.4 %copy-start.8 = (s32[128]{0:T(128)S(1)}, s32[128]{0:T(128)}, u32[]{:S(2)}) copy-start(s32[128]{0:T(128)} %param.26) | copy-start | bytes 1540
  7.2 8.1 %copy-start.1 = (bf16[128,2048]{1,0:T(8,128)(2,1)S(1)}, bf16[128,2048]{1,0:T(8,128)(2,1)}, u32[]{:S(2)}) copy-start(bf16[128,2048]{1,0:T(8,128)(2,1)} %param.24) | copy-start | bytes 1572868
  7.2 8.3 %copy-start.3 = (f32[2048]{0:T(1024)S(1)}, f32[2048]{0:T(1024)}, u32[]{:S(2)}) copy-start(f32[2048]{0:T(1024)} %param.25) | copy-start | bytes 24580
  7.2 71.8 %all-gather.7.cloned.1.call-start = ((), (), s32[]{:S(2)}) async-start(), calls=%async_computation.3 | async-start | bytes 2359296 | tf_op jit(solution)/shard_map/all_gather | solution.py:79
  9.1 122.8 %all-gather.9.cloned.1.call-start = ((), (), s32[]{:S(2)}) async-start(), calls=%async_computation.4 | async-start | bytes 2359296 | tf_op jit(solution)/shard_map/all_gather | solution.py:80
  11.0 158.5 %all-gather.13.cloned.1.call-start = ((), (), s32[]{:S(2)}) async-start(), calls=%async_computation.6 | async-start | bytes 5242880 | tf_op jit(solution)/shard_map/all_gather | solution.py:136
  11.7 191.9 %all-gather.17.cloned.1.call-start = ((), (), s32[]{:S(2)}) async-start(), calls=%async_computation.8 | async-start | bytes 5242880 | tf_op jit(solution)/shard_map/all_gather | solution.py:138
  12.3 12.1 %copy-start.2 = (bf16[512,256]{1,0:T(8,128)(2,1)S(1)}, bf16[512,256]{1,0:T(8,128)(2,1)}, u32[]{:S(2)}) copy-start(bf16[512,256]{1,0:T(8,128)(2,1)} %param.18) | copy-start | bytes 786436
  12.3 227.7 %all-gather.15.cloned.1.call-start = ((), (), s32[]{:S(2)}) async-start(), calls=%async_computation.7 | async-start | bytes 5242880 | tf_op jit(solution)/shard_map/all_gather | solution.py:137
  12.9 263.0 %all-gather.11.cloned.1.call-start = ((), (), s32[]{:S(2)}) async-start(), calls=%async_computation.5 | async-start | bytes 5242880 | tf_op jit(solution)/shard_map/all_gather | solution.py:139
  17.1 137.6 %all-to-all-start.1 = ((bf16[8,40,2048]{2,1,0:T(8,128)(2,1)}), bf16[8,40,2048]{2,1,0:T(8,128)(2,1)}, u32[]{:S(2)}, u32[]{:S(2)}) async-start(bf16[8,40,2048]{2,1,0:T(8,128)(2,1)} %bitcast.18), calls=%async_computation.1 | async-start | bytes 2621440 | tf_op jit(solution)/shard_map/all_to_all | solution.py:134
  132.1 20.8 %copy-start.6 = (f32[2]{0:T(128)S(1)}, f32[2]{0:T(128)}, u32[]{:S(2)}) copy-start(f32[2]{0:T(128)} %param.21) | copy-start | bytes 28
  132.1 21.3 %copy-start.7 = (f32[128]{0:T(128)S(1)}, f32[128]{0:T(128)}, u32[]{:S(2)}) copy-start(f32[128]{0:T(128)} %param.22) | copy-start | bytes 1540
  140.1 4.2 %copy-start = (bf16[256,4096]{1,0:T(8,128)(2,1)S(1)}, bf16[256,4096]{1,0:T(8,128)(2,1)}, u32[]{:S(2)}) copy-start(bf16[256,4096]{1,0:T(8,128)(2,1)} %get-tuple-element.318) | copy-start | bytes 6291460 | tf_op jit(solution)/shard_map/while/body/eval_jaxpr/cond
  154.8 93.3 %all-to-all-start = ((bf16[4,128,256]{2,1,0:T(8,128)(2,1)}), bf16[4,128,256]{2,1,0:T(8,128)(2,1)S(1)}, u32[]{:S(2)}, u32[]{:S(2)}) async-start(bf16[4,128,256]{2,1,0:T(8,128)(2,1)} %all_to_all.30), calls=%async_computation | async-start | bytes 524288 | tf_op jit(solution)/shard_map/all_to_all | solution.py:141
  173.6 80.1 %copy-start.5 = (f32[128,2]{0,1:T(2,128)S(1)}, f32[128,2]{0,1:T(2,128)}, u32[]{:S(2)}) copy-start(f32[128,2]{0,1:T(2,128)} %param.28) | copy-start | bytes 3076
  248.1 37.3 %all-to-all-start.2 = ((bf16[8,40,2048]{2,1,0:T(8,128)(2,1)}), bf16[8,40,2048]{2,1,0:T(8,128)(2,1)S(1)}, u32[]{:S(2)}, u32[]{:S(2)}) async-start(bf16[8,40,2048]{2,1,0:T(8,128)(2,1)} %bitcast.23), calls=%async_computation.2 | async-start | bytes 2621440 | tf_op jit(solution)/shard_map/all_to_all | solution.py:147
Sparse Core Ops, SparseCore 0:
  10.6 68.3 all-gather.6
  81.6 50.3 all-gather.8
  133.5 35.9 all-gather.12
  170.9 32.5 all-gather.16
  205.0 34.9 all-gather.14
  241.4 34.4 all-gather.10
where the time goes:
time: 299 us
  waiting for transfers between devices  215 us (72%)
  matrix products  28.9 us (10%)
  starting transfers between devices  16.5 us (6%)
  between operations  14.4 us (5%)
  local copies, waits for them, and re-layouts  11.6 us (4%)
  other arithmetic  10.7 us (4%)
    all_gather x1, waiting for transfers between devices, body(): key_piece = lax.all_gather(key_cols, 'ep', axis=1, tiled=True)  54.4 us
    all_gather x1, waiting for transfers between devices, body(): value_piece = lax.all_gather(value_cols, 'ep', axis=1, tiled=True)  53 us
    all_gather x1, waiting for transfers between devices, body(): lax.all_gather(up_weight, 'tp', axis=2, tiled=True)  36.4 us
    all_gather x1, waiting for transfers between devices, body(): lax.all_gather(down_weight, 'tp', axis=1, tiled=True)  29.9 us
    all_gather x1, waiting for transfers between devices, body(): lax.all_gather(out_weight, 'tp', axis=0, tiled=True)  21.9 us
    all_gather x1, waiting for transfers between devices, body(): lax.all_gather(gate_weight, 'tp', axis=2, tiled=True)  11.4 us
    dot_general x1, matrix products, body(): jnp.dot(hidden, down_all[0], preferred_element_type=jnp.float32)  8.05 us
    all_to_all x1, starting transfers between devices, body(): lax.all_to_all(outgoing, 'ep', split_axis=0, concat_axis=0, tiled=True)  7.31 us
  transfers between devices with their start and end apart: 9, of which 7 were waited for; matrix products, arithmetic and copies ran while one was open for 14% of the time, Pallas kernels for 0%

commit v1 on v0

--- a/solution.py
+++ b/solution.py
@@ -76,7 +76,12 @@
     init_state = tuple((initial(group[1].shape[0]) for group in query_groups))
     key_cols = key_rows.T
     value_cols = value_rows.T
-    key_piece = lax.all_gather(key_cols, "ep", axis=1, tiled=True)
+    ring = [key_cols]
+    for hop in range(7):
+        ring.append(lax.ppermute(ring[-1], "ep", [(dev, (dev + 1) % 8) for dev in range(8)]))
+    key_piece = jnp.roll(
+        jnp.concatenate(ring[::-1], axis=1), (lax.axis_index("ep") + 1) * ring[0].shape[1], axis=1
+    )
     value_piece = lax.all_gather(value_cols, "ep", axis=1, tiled=True)
     shard_count = key_piece.shape[1] // seg_rows
     stride = max(1, 2048 // seg_rows)

time: 299 us -> 246 us (0.82)
  waiting for transfers between devices: 215 us -> 152 us
  matrix products: 28.9 us -> 34 us
    ppermute x0 -> x7, waiting for transfers between devices: none -> 75.5 us  [body(): lax.ppermute(ring[-1], 'ep', [(dev, (dev + 1) % 8) for dev in range(8)])]
    all_gather x1 -> x0, waiting for transfers between devices: 54.4 us -> none  [body(): key_piece = lax.all_gather(key_cols, 'ep', axis=1, tiled=True)]
    all_gather x1, waiting for transfers between devices: 53 us -> 0.02 us  [body(): value_piece = lax.all_gather(value_cols, 'ep', axis=1, tiled=True)]
    all_gather x1, waiting for transfers between devices: 36.4 us -> 12.2 us  [body(): lax.all_gather(up_weight, 'tp', axis=2, tiled=True)]
    all_gather x1, waiting for transfers between devices: 11.4 us -> 0.02 us  [body(): lax.all_gather(gate_weight, 'tp', axis=2, tiled=True)]
    all_gather x1, waiting for transfers between devices: 29.9 us -> 34.1 us  [body(): lax.all_gather(down_weight, 'tp', axis=1, tiled=True)]
    dot_general x2, matrix products: 6.98 us -> 10.3 us  [one_map(): jnp.einsum('hqk,hdk->hqd', exps.astype(jnp.bfloat16), value_blk, preferre...]
    ppermute x0 -> x7, starting transfers between devices: none -> 3.06 us  [body(): lax.ppermute(ring[-1], 'ep', [(dev, (dev + 1) % 8) for dev in range(8)])]
  transfers between devices with their start and end apart: 9 -> 15, of which waited for: 7 -> 11; matrix products, arithmetic and copies ran while one was open for 14% -> 21% of each run, Pallas kernels for 0% -> 0%
where the time goes in v1:
time: 246 us
  waiting for transfers between devices  152 us (62%)
  matrix products  34 us (14%)
  starting transfers between devices  18.4 us (7%)
  between operations  14.2 us (6%)
  other arithmetic  13.1 us (5%)
  local copies, waits for them, and re-layouts  12.7 us (5%)
    ppermute x7, waiting for transfers between devices, body(): lax.ppermute(ring[-1], 'ep', [(dev, (dev + 1) % 8) for dev in range(8)])  75.5 us
    all_gather x1, waiting for transfers between devices, body(): lax.all_gather(down_weight, 'tp', axis=1, tiled=True)  34.1 us
    all_gather x1, waiting for transfers between devices, body(): lax.all_gather(out_weight, 'tp', axis=0, tiled=True)  22 us
    all_gather x1, waiting for transfers between devices, body(): lax.all_gather(up_weight, 'tp', axis=2, tiled=True)  12.2 us
    dot_general x2, matrix products, one_map(): jnp.einsum('hqk,hdk->hqd', exps.astype(jnp.bfloat16), value_blk, preferre...  10.3 us
    dot_general x1, matrix products, body(): jnp.dot(hidden, down_all[0], preferred_element_type=jnp.float32)  7.92 us
    dot_general x2, matrix products, one_map(): jnp.einsum('hqd,hdk->hqk', query_map, key_map, preferred_element_type=jnp...  6.15 us
    all_to_all x1, starting transfers between devices, body(): lax.all_to_all(outgoing, 'ep', split_axis=0, concat_axis=0, tiled=True)  6 us
  transfers between devices with their start and end apart: 15, of which 11 were waited for; matrix products, arithmetic and copies ran while one was open for 21% of the time, Pallas kernels for 0%

profile of v1, /device:TPU:0, one launch (start us, length us, event | category | flops | bytes accessed | tf_op | source)
XLA Modules:
  0.0 245.9 jit_solution(15155421204649499192)
XLA Ops:
  7.3 1.8 copy.40
  11.2 1.1 copy.38
  12.3 3.0 %collective-permute-start = (bf16[256,512]{1,0:T(8,128)(2,1)S(1)}, bf16[256,512]{1,0:T(8,128)(2,1)S(1)}, u32[]{:S(2)}, u32[]{:S(2)}) collective-permute-start(bf16[256,512]{1,0:T(8,128)(2,1)S(1)} %bitcast.103), channel_id=1, source_target_pairs={{0,4},{4,8},{8,12},{12,16},{16,20},{20,24},{24,28},{28,0},{1,5},{5... | collective-permute-start | bytes 786440 | tf_op jit(solution)/shard_map/ppermute | solution.py:81
  15.3 9.4 %collective-permute-done = bf16[256,512]{1,0:T(8,128)(2,1)S(1)} collective-permute-done((bf16[256,512]{1,0:T(8,128)(2,1)S(1)}, bf16[256,512]{1,0:T(8,128)(2,1)S(1)}, u32[]{:S(2)}, u32[]{:S(2)}) %collective-permute-start) | collective-permute-done | bytes 262176 | tf_op jit(solution)/shard_map/ppermute | solution.py:81
  24.8 13.9 %collective-permute-done.1 = bf16[256,512]{1,0:T(8,128)(2,1)S(1)} collective-permute-done((bf16[256,512]{1,0:T(8,128)(2,1)S(1)}, bf16[256,512]{1,0:T(8,128)(2,1)S(1)}, u32[]{:S(2)}, u32[]{:S(2)}) %collective-permute-start.1) | collective-permute-done | bytes 262176 | tf_op jit(solution)/shard_map/ppermute | solution.py:81
  39.7 8.1 %collective-permute-done.2 = bf16[256,512]{1,0:T(8,128)(2,1)S(1)} collective-permute-done((bf16[256,512]{1,0:T(8,128)(2,1)S(1)}, bf16[256,512]{1,0:T(8,128)(2,1)S(1)}, u32[]{:S(2)}, u32[]{:S(2)}) %collective-permute-start.2) | collective-permute-done | bytes 262176 | tf_op jit(solution)/shard_map/ppermute | solution.py:81
  49.0 14.7 %collective-permute-done.3 = bf16[256,512]{1,0:T(8,128)(2,1)S(1)} collective-permute-done((bf16[256,512]{1,0:T(8,128)(2,1)S(1)}, bf16[256,512]{1,0:T(8,128)(2,1)S(1)}, u32[]{:S(2)}, u32[]{:S(2)}) %collective-permute-start.3) | collective-permute-done | bytes 262176 | tf_op jit(solution)/shard_map/ppermute | solution.py:81
  64.0 15.3 %collective-permute-done.4 = bf16[256,512]{1,0:T(8,128)(2,1)S(1)} collective-permute-done((bf16[256,512]{1,0:T(8,128)(2,1)S(1)}, bf16[256,512]{1,0:T(8,128)(2,1)S(1)}, u32[]{:S(2)}, u32[]{:S(2)}) %collective-permute-start.4) | collective-permute-done | bytes 262176 | tf_op jit(solution)/shard_map/ppermute | solution.py:81
  79.4 11.3 %collective-permute-done.5 = bf16[256,512]{1,0:T(8,128)(2,1)S(1)} collective-permute-done((bf16[256,512]{1,0:T(8,128)(2,1)S(1)}, bf16[256,512]{1,0:T(8,128)(2,1)S(1)}, u32[]{:S(2)}, u32[]{:S(2)}) %collective-permute-start.5) | collective-permute-done | bytes 262176 | tf_op jit(solution)/shard_map/ppermute | solution.py:81
  90.7 1.7 convolution_convert_fusion
  92.3 6.0 %all-to-all-start.1 = ((bf16[8,40,2048]{2,1,0:T(8,128)(2,1)}), bf16[8,40,2048]{2,1,0:T(8,128)(2,1)}, u32[]{:S(2)}, u32[]{:S(2)}) async-start(bf16[8,40,2048]{2,1,0:T(8,128)(2,1)} %bitcast.18), calls=%async_computation.1 | async-start | bytes 2621440 | tf_op jit(solution)/shard_map/all_to_all | solution.py:139
  99.8 2.7 %collective-permute-done.6 = bf16[256,512]{1,0:T(8,128)(2,1)S(1)} collective-permute-done((bf16[256,512]{1,0:T(8,128)(2,1)S(1)}, bf16[256,512]{1,0:T(8,128)(2,1)S(1)}, u32[]{:S(2)}, u32[]{:S(2)}) %collective-permute-start.6) | collective-permute-done | bytes 262176 | tf_op jit(solution)/shard_map/ppermute | solution.py:81
  105.0 24.5 %while.23 = (s32[]{:T(128)}, f32[2,512]{1,0:T(2,128)S(1)}, f32[2,512]{1,0:T(2,128)S(1)}, f32[2,512,128]{2,1,0:T(8,128)}, f32[2,512]{1,0:T(2,128)S(1)}, /*index=5...) while((s32[]{:T(128)}, f32[2,512]{1,0:T(2,128)S(1)}, ...), condition=%wide.region_7.8_spmd, body=%wide.region_0.7_spmd.sunk | while | flops 1666717696 | bytes 82201000 | solution.py:113
  106.5 21.7 %conditional.2 = ((f32[2,512]{1,0:T(2,128)S(1)}, f32[2,512]{1,0:T(2,128)S(1)}, f32[2,512,128]{2,1,0:T(8,128)}, f32[2,512]{1,0:T(2,128)S(1)}, f32[2,512]{1,0:T(2,128)S(1)}, /*index=5*/f32[2,512,128]{2,1,0:T(8,128)})) conditional(s32[]{:T(128)} %convert_element_type.97, (f32[2,512]{1,0:T(2,128)S(1)}, f32[2,512]{1,0:T(2,128)S(1)}, ...), branch_computations={%region_1.1_spmd, %region_2.6_spmd} | conditional | flops 1666717696 | bytes 82200704 | solution.py:109
  106.6 2.2 fusion.19
  109.6 4.0 %fusion.1 = (f32[2,512]{1,0:T(2,128)S(1)}, f32[2,512]{1,0:T(2,128)S(1)}, f32[2,2048,512]{2,1,0:T(8,128)S(1)}) fusion(pred[512,2048]{0,1:T(8,128)(4,1)S(1)} %broadcast_compare_fusion, f32[2,2048,512]{2,1,0:T(8,128)S(1)} %fusion.19, bf16[2,2,512,64]{2,3,0,1:T(8,128)(2,1)} %get-tuple-element.315, bf16[2,2,64,2048]{3,2,1,0:T(8,128)(2,1)S(1)} %bitcast.100), kind=kOutput, calls=%fused_computation.6 | convolution fusion | flops 281016320 | bytes 18489344 | tf_op jit(solution)/shard_map/while/body/eval_jaxpr/cond/branch_1_fun/hqd,hdk->hqk/dot_general | solution.py:50
  113.6 4.1 %fusion.5 = (f32[2,512]{1,0:T(2,128)S(1)}, f32[2,512]{1,0:T(2,128)S(1)}) fusion(f32[2,2048,512]{2,1,0:T(8,128)S(1)} %get-tuple-element.406, f32[2,512]{1,0:T(2,128)S(1)} %max.11, pred[512,2048]{0,1:T(8,128)(4,1)S(1)} %broadcast_compare_fusion, f32[2,512]{1,0:T(2,128)S(1)} %max.10, f32[2,2048,512]{2,1,0:T(8,128)S(1)} %fusion.19), kind=kLoop, calls=%fused_computation.10 | loop fusion | flops 20969472 | bytes 17842176 | tf_op jit(solution)/shard_map/while/body/eval_jaxpr/cond/branch_1_fun/reduce_sum | solution.py:57
  117.9 5.1 %fusion.15 = f32[2,512,128]{2,1,0:T(8,128)} fusion(bf16[2,128,2048]{2,1,0:T(8,128)(2,1)S(1)} %bitcast.101, f32[2,2048,512]{2,1,0:T(8,128)S(1)} %get-tuple-element.406, f32[2,512]{1,0:T(2,128)S(1)} %max.11, pred[512,2048]{0,1:T(8,128)(4,1)S(1)} %broadcast_compare_fusion, f32[2,512,128]{2,1,0:T(8,128)} %get-tuple-element.321, f32[2,512]{1,0:T(2,128)S(1)} %get-tuple-element.399), kind=kOutput, calls=%fused_computation.17 | convolution fusion | flops 547618816 | bytes 11542528 | tf_op jit(solution)/shard_map/while/body/eval_jaxpr/cond/branch_1_fun/hqk,hdk->hqd/dot_general | solution.py:58
  123.0 5.1 %fusion.12 = f32[2,512,128]{2,1,0:T(8,128)} fusion(bf16[2,128,2048]{2,1,0:T(8,128)(2,1)S(1)} %bitcast.102, f32[2,2048,512]{2,1,0:T(8,128)S(1)} %fusion.19, f32[2,512]{1,0:T(2,128)S(1)} %max.10, pred[512,2048]{0,1:T(8,128)(4,1)S(1)} %broadcast_compare_fusion, f32[2,512,128]{2,1,0:T(8,128)} %get-tuple-element.317, f32[2,512]{1,0:T(2,128)S(1)} %get-tuple-element.408), kind=kOutput, calls=%fused_computation.16 | convolution fusion | flops 547618816 | bytes 11542528 | tf_op jit(solution)/shard_map/while/body/eval_jaxpr/cond/branch_1_fun/hqk,hdk->hqd/dot_general | solution.py:58
  129.5 1.7 multiply_reduce_fusion.1
  133.2 3.6 %all-to-all-start = ((bf16[4,128,256]{2,1,0:T(8,128)(2,1)}), bf16[4,128,256]{2,1,0:T(8,128)(2,1)S(1)}, u32[]{:S(2)}, u32[]{:S(2)}) async-start(bf16[4,128,256]{2,1,0:T(8,128)(2,1)} %all_to_all.30), calls=%async_computation | async-start | bytes 524288 | tf_op jit(solution)/shard_map/all_to_all | solution.py:146
  136.9 4.3 %fusion.34 = f32[320,1024]{1,0:T(8,128)S(1)} fusion(bf16[320,2048]{1,0:T(8,128)(2,1)} %bitcast.19, bf16[1,2048,1024]{2,1,0:T(8,128)(2,1)} %all-gather.10.cloned.1.call-done), kind=kOutput, calls=%fused_computation.43 | convolution fusion | flops 1342177280 | bytes 6815744 | tf_op jit(solution)/shard_map/dot_general | solution.py:148
  141.2 12.2 %all-gather.12.cloned.1.call-done = bf16[1,2048,1024]{2,1,0:T(8,128)(2,1)} async-done(((bf16[1,2048,256]{2,1,0:T(8,128)(2,1)}), bf16[1,2048,1024]{2,1,0:T(8,128)(2,1)}) %all-gather.12.cloned.1.call-update) | async-done | bytes 4194320 | tf_op jit(solution)/shard_map/all_gather | solution.py:142
  153.4 34.1 %all-gather.14.cloned.1.call-done = bf16[1,1024,2048]{2,1,0:T(8,128)(2,1)} async-done(((bf16[1,256,2048]{2,1,0:T(8,128)(2,1)}), bf16[1,1024,2048]{2,1,0:T(8,128)(2,1)}) %all-gather.14.cloned.1.call-update) | async-done | bytes 4194320 | tf_op jit(solution)/shard_map/all_gather | solution.py:143
  187.5 7.9 %fusion.36 = bf16[320,2048]{1,0:T(8,128)(2,1)} fusion(bf16[1,1024,2048]{2,1,0:T(8,128)(2,1)} %all-gather.14.cloned.1.call-done, bf16[320,2048]{1,0:T(8,128)(2,1)} %bitcast.19, bf16[1,2048,1024]{2,1,0:T(8,128)(2,1)} %all-gather.12.cloned.1.call-done, f32[320,1024]{1,0:T(8,128)S(1)} %fusion.34), kind=kOutput, calls=%fused_computation.46 | convolution fusion | flops 2686976000 | bytes 12320768 | tf_op jit(solution)/shard_map/dot_general | solution.py:151
  195.4 5.5 %all-to-all-start.2 = ((bf16[8,40,2048]{2,1,0:T(8,128)(2,1)}), bf16[8,40,2048]{2,1,0:T(8,128)(2,1)S(1)}, u32[]{:S(2)}, u32[]{:S(2)}) async-start(bf16[8,40,2048]{2,1,0:T(8,128)(2,1)} %bitcast.23), calls=%async_computation.2 | async-start | bytes 2621440 | tf_op jit(solution)/shard_map/all_to_all | solution.py:152
  201.4 22.0 %all-gather.8.cloned.1.call-done = bf16[1024,2048]{1,0:T(8,128)(2,1)} async-done(((bf16[256,2048]{1,0:T(8,128)(2,1)}), bf16[1024,2048]{1,0:T(8,128)(2,1)}) %all-gather.8.cloned.1.call-update) | async-done | bytes 4194320 | tf_op jit(solution)/shard_map/all_gather | solution.py:144
  223.4 3.7 %convolution_convert_fusion.1 = bf16[128,2048]{1,0:T(8,128)(2,1)} fusion(bf16[128,1024]{0,1:T(8,128)(2,1)S(1)} %bitcast.104, bf16[1024,2048]{1,0:T(8,128)(2,1)} %all-gather.8.cloned.1.call-done), kind=kOutput, calls=%fused_computation.47 | convolution fusion | flops 537133056 | bytes 4980736 | tf_op jit(solution)/shard_map/dot_general | solution.py:147
  227.1 5.6 %all-to-all-done.2 = bf16[8,40,2048]{2,1,0:T(8,128)(2,1)S(1)} async-done(((bf16[8,40,2048]{2,1,0:T(8,128)(2,1)}), bf16[8,40,2048]{2,1,0:T(8,128)(2,1)S(1)}, u32[]{:S(2)}, u32[]{:S(2)}) %all-to-all-start.2) | async-done | bytes 1310752 | tf_op jit(solution)/shard_map/all_to_all | solution.py:152
  232.7 1.4 gather_fusion
  234.1 1.3 reshape.164
  235.4 3.9 %multiply_reduce_fusion = bf16[128,2048]{1,0:T(8,128)(2,1)} fusion(f32[128,2,2048]{2,1,0:T(2,128)S(1)} %reshape.164, f32[128,2]{1,0:T(8,128)S(1)} %copy.46), kind=kLoop, calls=%fused_computation.48 | loop fusion | flops 786432 | bytes 2622464 | tf_op jit(solution)/shard_map/reduce_sum | solution.py:154
  (100 shorter events, 13.1 us)
Async XLA Ops:
  7.2 31.5 %copy-start.7 = (s32[128]{0:T(128)S(1)}, s32[128]{0:T(128)}, u32[]{:S(2)}) copy-start(s32[128]{0:T(128)} %param.26) | copy-start | bytes 1540
  7.2 31.5 %copy-start.5 = (s32[128,2]{0,1:T(2,128)S(1)}, s32[128,2]{0,1:T(2,128)}, u32[]{:S(2)}) copy-start(s32[128,2]{0,1:T(2,128)} %param.27) | copy-start | bytes 3076
  7.2 56.6 %copy-start.1 = (bf16[128,2048]{1,0:T(8,128)(2,1)S(1)}, bf16[128,2048]{1,0:T(8,128)(2,1)}, u32[]{:S(2)}) copy-start(bf16[128,2048]{1,0:T(8,128)(2,1)} %param.24) | copy-start | bytes 1572868
  7.2 83.5 %copy-start.4 = (f32[2048]{0:T(1024)S(1)}, f32[2048]{0:T(1024)}, u32[]{:S(2)}) copy-start(f32[2048]{0:T(1024)} %param.25) | copy-start | bytes 24580
  7.2 96.1 %all-gather.6.cloned.1.call-start = ((), (), s32[]{:S(2)}) async-start(), calls=%async_computation.3 | async-start | bytes 2359296 | tf_op jit(solution)/shard_map/all_gather | solution.py:85
  9.1 127.8 %all-gather.10.cloned.1.call-start = ((), (), s32[]{:S(2)}) async-start(), calls=%async_computation.5 | async-start | bytes 5242880 | tf_op jit(solution)/shard_map/all_gather | solution.py:141
  9.9 143.5 %all-gather.12.cloned.1.call-start = ((), (), s32[]{:S(2)}) async-start(), calls=%async_computation.6 | async-start | bytes 5242880 | tf_op jit(solution)/shard_map/all_gather | solution.py:142
  10.6 88.3 %copy-start.3 = (bf16[512,256]{1,0:T(8,128)(2,1)S(1)}, bf16[512,256]{1,0:T(8,128)(2,1)}, u32[]{:S(2)}) copy-start(bf16[512,256]{1,0:T(8,128)(2,1)} %param.18) | copy-start | bytes 786436
  10.6 176.9 %all-gather.14.cloned.1.call-start = ((), (), s32[]{:S(2)}) async-start(), calls=%async_computation.7 | async-start | bytes 5242880 | tf_op jit(solution)/shard_map/all_gather | solution.py:143
  12.3 12.5 %collective-permute-start = (bf16[256,512]{1,0:T(8,128)(2,1)S(1)}, bf16[256,512]{1,0:T(8,128)(2,1)S(1)}, u32[]{:S(2)}, u32[]{:S(2)}) collective-permute-start(bf16[256,512]{1,0:T(8,128)(2,1)S(1)} %bitcast.103), channel_id=1, source_target_pairs={{0,4},{4,8},{8,12},{12,16},{16,20},{20,24},{24,28},{28,0},{1,5},{5... | collective-permute-start | bytes 786440 | tf_op jit(solution)/shard_map/ppermute | solution.py:81
  24.8 13.9 %collective-permute-start.1 = (bf16[256,512]{1,0:T(8,128)(2,1)S(1)}, bf16[256,512]{1,0:T(8,128)(2,1)S(1)}, u32[]{:S(2)}, u32[]{:S(2)}) collective-permute-start(bf16[256,512]{1,0:T(8,128)(2,1)S(1)} %collective-permute-done), channel_id=1, source_target_pairs={{0,4},{4,8},{8,12},{12,16},{16,20},{20,24},{24,28},{28,0},{1,5},{5... | collective-permute-start | bytes 786440 | tf_op jit(solution)/shard_map/ppermute | solution.py:81
  38.7 9.1 %collective-permute-start.2 = (bf16[256,512]{1,0:T(8,128)(2,1)S(1)}, bf16[256,512]{1,0:T(8,128)(2,1)S(1)}, u32[]{:S(2)}, u32[]{:S(2)}) collective-permute-start(bf16[256,512]{1,0:T(8,128)(2,1)S(1)} %collective-permute-done.1), channel_id=1, source_target_pairs={{0,4},{4,8},{8,12},{12,16},{16,20},{20,24},{24,28},{28,0},{1,5},{5... | collective-permute-start | bytes 786440 | tf_op jit(solution)/shard_map/ppermute | solution.py:81
  47.8 16.0 %collective-permute-start.3 = (bf16[256,512]{1,0:T(8,128)(2,1)S(1)}, bf16[256,512]{1,0:T(8,128)(2,1)S(1)}, u32[]{:S(2)}, u32[]{:S(2)}) collective-permute-start(bf16[256,512]{1,0:T(8,128)(2,1)S(1)} %collective-permute-done.2), channel_id=1, source_target_pairs={{0,4},{4,8},{8,12},{12,16},{16,20},{20,24},{24,28},{28,0},{1,5},{5... | collective-permute-start | bytes 786440 | tf_op jit(solution)/shard_map/ppermute | solution.py:81
  63.7 15.6 %collective-permute-start.4 = (bf16[256,512]{1,0:T(8,128)(2,1)S(1)}, bf16[256,512]{1,0:T(8,128)(2,1)S(1)}, u32[]{:S(2)}, u32[]{:S(2)}) collective-permute-start(bf16[256,512]{1,0:T(8,128)(2,1)S(1)} %collective-permute-done.3), channel_id=1, source_target_pairs={{0,4},{4,8},{8,12},{12,16},{16,20},{20,24},{24,28},{28,0},{1,5},{5... | collective-permute-start | bytes 786440 | tf_op jit(solution)/shard_map/ppermute | solution.py:81
  79.3 11.3 %collective-permute-start.5 = (bf16[256,512]{1,0:T(8,128)(2,1)S(1)}, bf16[256,512]{1,0:T(8,128)(2,1)S(1)}, u32[]{:S(2)}, u32[]{:S(2)}) collective-permute-start(bf16[256,512]{1,0:T(8,128)(2,1)S(1)} %collective-permute-done.4), channel_id=1, source_target_pairs={{0,4},{4,8},{8,12},{12,16},{16,20},{20,24},{24,28},{28,0},{1,5},{5... | collective-permute-start | bytes 786440 | tf_op jit(solution)/shard_map/ppermute | solution.py:81
  90.7 11.9 %collective-permute-start.6 = (bf16[256,512]{1,0:T(8,128)(2,1)S(1)}, bf16[256,512]{1,0:T(8,128)(2,1)S(1)}, u32[]{:S(2)}, u32[]{:S(2)}) collective-permute-start(bf16[256,512]{1,0:T(8,128)(2,1)S(1)} %collective-permute-done.5), channel_id=1, source_target_pairs={{0,4},{4,8},{8,12},{12,16},{16,20},{20,24},{24,28},{28,0},{1,5},{5... | collective-permute-start | bytes 786440 | tf_op jit(solution)/shard_map/ppermute | solution.py:81
  92.3 40.9 %all-to-all-start.1 = ((bf16[8,40,2048]{2,1,0:T(8,128)(2,1)}), bf16[8,40,2048]{2,1,0:T(8,128)(2,1)}, u32[]{:S(2)}, u32[]{:S(2)}) async-start(bf16[8,40,2048]{2,1,0:T(8,128)(2,1)} %bitcast.18), calls=%async_computation.1 | async-start | bytes 2621440 | tf_op jit(solution)/shard_map/all_to_all | solution.py:139
  98.3 125.1 %all-gather.8.cloned.1.call-start = ((), (), s32[]{:S(2)}) async-start(), calls=%async_computation.4 | async-start | bytes 5242880 | tf_op jit(solution)/shard_map/all_gather | solution.py:144
  113.6 4.2 %copy-start = (bf16[256,4096]{1,0:T(8,128)(2,1)S(1)}, bf16[256,4096]{1,0:T(8,128)(2,1)}, u32[]{:S(2)}) copy-start(bf16[256,4096]{1,0:T(8,128)(2,1)} %get-tuple-element.318) | copy-start | bytes 6291460 | tf_op jit(solution)/shard_map/while/body/eval_jaxpr/cond
  133.2 62.2 %all-to-all-start = ((bf16[4,128,256]{2,1,0:T(8,128)(2,1)}), bf16[4,128,256]{2,1,0:T(8,128)(2,1)S(1)}, u32[]{:S(2)}, u32[]{:S(2)}) async-start(bf16[4,128,256]{2,1,0:T(8,128)(2,1)} %all_to_all.30), calls=%async_computation | async-start | bytes 524288 | tf_op jit(solution)/shard_map/all_to_all | solution.py:146
  141.2 59.8 %copy-start.2 = (s32[128,2]{1,0:T(8,128)S(1)}, s32[128,2]{1,0:T(8,128)}, u32[]{:S(2)}) copy-start(s32[128,2]{1,0:T(8,128)} %get-tuple-element.402) | copy-start | bytes 3076
  141.2 59.9 %copy-start.6 = (f32[128,2]{0,1:T(2,128)S(1)}, f32[128,2]{0,1:T(2,128)}, u32[]{:S(2)}) copy-start(f32[128,2]{0,1:T(2,128)} %param.28) | copy-start | bytes 3076
  195.4 37.3 %all-to-all-start.2 = ((bf16[8,40,2048]{2,1,0:T(8,128)(2,1)}), bf16[8,40,2048]{2,1,0:T(8,128)(2,1)S(1)}, u32[]{:S(2)}, u32[]{:S(2)}) async-start(bf16[8,40,2048]{2,1,0:T(8,128)(2,1)} %bitcast.23), calls=%async_computation.2 | async-start | bytes 2621440 | tf_op jit(solution)/shard_map/all_to_all | solution.py:152
Sparse Core Ops, SparseCore 0:
  10.6 65.6 all-gather.5
  77.9 36.0 all-gather.9
  115.6 37.7 all-gather.11
  154.8 32.6 all-gather.13
  188.9 34.4 all-gather.7
